TPU v7x, 32 devices: a whole 2x2x4 slice. The times are simulated.
32 devices in a mesh: sp: 8 (over z, y), tp: 4 (over x, core).
Axes of the slice: x: 2, y: 2, z: 4, core: 2. Of those that a mesh axis runs over, the one named last changes fastest.
Arguments:
- tokens: bfloat16 [3072, 2048], P('sp', 'tp'), may hold values from -6 to 6
- norm_gain: float32 [2048], replicated, may hold values from 0.1 to 1.9
- w_query_down: bfloat16 [2048, 512], replicated, may hold values from -0.125 to 0.125
- query_gain: float32 [512], replicated, may hold values from 0.1 to 1.9
- w_query_up: bfloat16 [512, 1536], P(None, 'tp'), may hold values from -0.25 to 0.25
- w_latent_down: bfloat16 [2048, 256], replicated, may hold values from -0.125 to 0.125
- latent_gain: float32 [256], replicated, may hold values from 0.1 to 1.9
- w_rotary_key: bfloat16 [2048, 32], replicated, may hold values from -0.125 to 0.125
- w_latent_up: bfloat16 [256, 2048], P(None, 'tp'), may hold values from -0.375 to 0.375
- query_head_gain: float32 [96], replicated, may hold values from 0.1 to 1.9
- key_head_gain: float32 [96], replicated, may hold values from 0.1 to 1.9
- w_pool_in: bfloat16 [2048, 1024], P(None, 'tp'), may hold values from -0.125 to 0.125
- w_pool_mix: bfloat16 [4, 256, 256], P('tp'), may hold values from -0.375 to 0.375
- pool_scale: float32 [1024], P('tp'), may hold values from 0.1 to 1.9
- w_attn_out: bfloat16 [1024, 2048], P('tp'), may hold values from -12 to 12
- w_pool_out: bfloat16 [1024, 2048], P('tp'), may hold values from -0.5 to 0.5
- w_gate_attn: bfloat16 [2048, 2048], P(None, 'tp'), may hold values from -0.125 to 0.125
- w_gate_pool: bfloat16 [2048, 2048], P(None, 'tp'), may hold values from -0.125 to 0.125
Outputs:
- mixed: bfloat16 [3072, 2048], P('sp', 'tp')
All inputs are finite; a program needn't handle non-finite values.
Results may differ from a plain program's by a relative error of at most 0.02.
Values may be sent and summed in bfloat16 or wider, within the bound.
A program may use at most 128 MiB of HBM per device.

v0:
```python
import jax
import jax.numpy as jnp
from jax import lax
from jax.sharding import PartitionSpec as P

NOPE = 64
ROPE = 32
VALUE_DIM = 64
POOL_GROUPS = 4
POOL_GROUP = 256
eps = 1e-06
theta = 10000.0


def extended(cells, sides, width):
    for axis, dim in sides:
        count = lax.axis_size(axis)
        ends = count - 1
        head = lax.slice_in_dim(cells, 0, width, axis=dim)
        tail = lax.slice_in_dim(cells, cells.shape[dim] - width, cells.shape[dim], axis=dim)
        cells = jnp.concatenate(
            [
                lax.ppermute(tail, axis, [(i, (i + 1) % count) for i in range(ends)]),
                cells,
                lax.ppermute(head, axis, [((i + 1) % count, i) for i in range(ends)]),
            ],
            axis=dim,
        )
    return cells


def rms_scale(values, gain):
    values = values.astype(jnp.float32)
    return values * lax.rsqrt(jnp.mean(values * values, axis=-1, keepdims=True) + eps) * gain


def rotate(values, positions):
    half = values.shape[-1] // 2
    freqs = theta ** (-jnp.arange(half, dtype=jnp.float32) / half)
    angles = positions.astype(jnp.float32)[:, None] * freqs[None, :]
    cosine = jnp.cos(angles)[:, None, :]
    sine = jnp.sin(angles)[:, None, :]
    first = values[..., :half]
    second = values[..., half:]
    return jnp.concatenate(
        [first * cosine - second * sine, first * sine + second * cosine], axis=-1
    )


def head_finish(values, gain, positions):
    normed = rms_scale(values, gain)
    return jnp.concatenate([normed[..., :NOPE], rotate(normed[..., NOPE:], positions)], axis=-1)


def body(
    tokens,
    norm_gain,
    w_query_down,
    query_gain,
    w_query_up,
    w_latent_down,
    latent_gain,
    w_rotary_key,
    w_latent_up,
    query_head_gain,
    key_head_gain,
    w_pool_in,
    w_pool_mix,
    pool_scale,
    w_attn_out,
    w_pool_out,
    w_gate_attn,
    w_gate_pool,
):
    bf = jnp.bfloat16
    rows = tokens.shape[0]
    length = rows * lax.axis_size("sp")
    local_heads = w_query_up.shape[1] // (NOPE + ROPE)
    positions = lax.axis_index("sp") * rows + jnp.arange(rows, dtype=jnp.int32)
    whole = lax.all_gather(tokens, "tp", axis=1, tiled=True)
    normed = rms_scale(whole, norm_gain).astype(bf)
    query_latent = jnp.dot(normed, w_query_down, preferred_element_type=jnp.float32).astype(bf)
    query_normed = rms_scale(query_latent, query_gain).astype(bf)
    query_raw = jnp.dot(query_normed, w_query_up, preferred_element_type=jnp.float32).astype(bf)
    query_raw = query_raw.reshape(rows, local_heads, NOPE + ROPE)
    query = (head_finish(query_raw, query_head_gain, positions) * (NOPE + ROPE) ** (-0.5)).astype(
        bf
    )
    latent = jnp.dot(normed, w_latent_down, preferred_element_type=jnp.float32).astype(bf)
    key_latent = rms_scale(latent, latent_gain).astype(bf)
    rotary_key = jnp.dot(normed, w_rotary_key, preferred_element_type=jnp.float32).astype(bf)
    start_state = (
        jnp.full((local_heads, rows), -1e30, jnp.float32),
        jnp.zeros((local_heads, rows), jnp.float32),
        jnp.zeros((local_heads, rows, VALUE_DIM), jnp.float32),
    )
    latent_piece = lax.all_gather(key_latent, "sp", axis=0, tiled=True)
    rotary_piece = lax.all_gather(rotary_key, "sp", axis=0, tiled=True)
    blocks = latent_piece.shape[0] // rows
    latent_blocks = latent_piece.reshape(blocks, rows, latent_piece.shape[1])
    rotary_blocks = rotary_piece.reshape(blocks, rows, rotary_piece.shape[1])

    def one_block(state, items):
        latent_block, rotary_block, number = items
        top, total, summed = state
        key_positions = number * rows + jnp.arange(rows, dtype=jnp.int32)
        keys_values = jnp.dot(latent_block, w_latent_up, preferred_element_type=jnp.float32).astype(
            bf
        )
        keys_values = keys_values.reshape(rows, local_heads, NOPE + VALUE_DIM)
        key_raw = jnp.concatenate(
            [
                keys_values[..., :NOPE],
                jnp.broadcast_to(rotary_block[:, None, :], (rows, local_heads, ROPE)),
            ],
            axis=-1,
        )
        key = head_finish(key_raw, key_head_gain, key_positions).astype(bf)
        values = keys_values[..., NOPE:]
        scores = jnp.einsum("qhd,khd->hqk", query, key, preferred_element_type=jnp.float32)
        new_top = jnp.maximum(top, jnp.max(scores, axis=-1))
        factor = jnp.exp(top - new_top)
        expo = jnp.exp(scores - new_top[..., None])
        total = total * factor + jnp.sum(expo, axis=-1)
        summed = summed * factor[..., None] + jnp.einsum(
            "hqk,khv->hqv", expo.astype(bf), values, preferred_element_type=jnp.float32
        )
        return ((new_top, total, summed), None)

    state, _ = lax.scan(
        one_block, start_state, (latent_blocks, rotary_blocks, jnp.arange(blocks, dtype=jnp.int32))
    )
    top, total, summed = state
    attn_rows = jnp.transpose(summed / total[..., None], (1, 0, 2)).reshape(
        rows, local_heads * VALUE_DIM
    )
    attn_rows = attn_rows.astype(bf)
    pool_input = jnp.dot(normed, w_pool_in, preferred_element_type=jnp.float32).astype(bf)
    reach = 2**POOL_GROUPS // 2
    padded = extended(pool_input, (("sp", 0),), reach).astype(jnp.float32)
    local_groups = w_pool_mix.shape[0]
    group_ids = lax.axis_index("tp") * local_groups + jnp.arange(local_groups, dtype=jnp.int32)
    windows = jnp.power(2, group_ids + 1)
    channel_window = jnp.repeat(windows, POOL_GROUP)
    pooled = jnp.zeros((rows, local_groups * POOL_GROUP), jnp.float32)
    for shift in range(-reach, reach):
        inside = (shift >= -(channel_window // 2)) & (
            shift <= channel_window - channel_window // 2 - 1
        )
        pooled = pooled + jnp.where(
            inside[None, :], padded[reach + shift : reach + shift + rows], 0.0
        )
    low = jnp.clip(positions[:, None] - channel_window[None, :] // 2, 0, length)
    high = jnp.clip(
        positions[:, None] + channel_window[None, :] - channel_window[None, :] // 2, 0, length
    )
    count = (high - low).astype(jnp.float32)
    pool_mixed = (pooled / count - pool_input.astype(jnp.float32)).astype(bf)
    pool_mixed = pool_mixed.reshape(rows, local_groups, POOL_GROUP)
    grouped = jnp.einsum("lgc,gcd->lgd", pool_mixed, w_pool_mix, preferred_element_type=jnp.float32)
    pool_rows = (grouped.reshape(rows, local_groups * POOL_GROUP) * pool_scale).astype(bf)
    gate_attn = jax.nn.sigmoid(jnp.dot(normed, w_gate_attn, preferred_element_type=jnp.float32))
    gate_pool = jax.nn.sigmoid(jnp.dot(normed, w_gate_pool, preferred_element_type=jnp.float32))
    attn_tokens, pool_tokens = (
        lax.all_to_all(attn_rows, "tp", split_axis=0, concat_axis=1, tiled=True),
        lax.all_to_all(pool_rows, "tp", split_axis=0, concat_axis=1, tiled=True),
    )
    attn_weight, pool_weight = (
        lax.all_gather(w_attn_out, "tp", axis=0, tiled=True),
        lax.all_gather(w_pool_out, "tp", axis=0, tiled=True),
    )
    attn_here = jnp.dot(attn_tokens, attn_weight, preferred_element_type=jnp.float32)
    pool_here = jnp.dot(pool_tokens, pool_weight, preferred_element_type=jnp.float32)
    attn_branch, pool_branch = (
        lax.all_to_all(
            attn_here.astype(jnp.bfloat16), "tp", split_axis=1, concat_axis=0, tiled=True
        ).astype(attn_here.dtype),
        lax.all_to_all(
            pool_here.astype(jnp.bfloat16), "tp", split_axis=1, concat_axis=0, tiled=True
        ).astype(pool_here.dtype),
    )
    return (gate_attn * attn_branch + gate_pool * pool_branch).astype(bf)


def solution(mesh):
    placed = (
        P("sp", "tp"),
        P(),
        P(),
        P(),
        P(None, "tp"),
        P(),
        P(),
        P(),
        P(None, "tp"),
        P(),
        P(),
        P(None, "tp"),
        P("tp", None, None),
        P("tp"),
        P("tp", None),
        P("tp", None),
        P(None, "tp"),
        P(None, "tp"),
    )
    return jax.shard_map(body, mesh=mesh, in_specs=placed, out_specs=P("sp", "tp"), check_vma=False)
```

profile of v0, /device:TPU:0, one launch (start us, length us, event | category | flops | bytes accessed | tf_op | source)
XLA Modules:
  0.0 212.7 jit_solution(344831506499883668)
XLA Ops:
  7.3 24.0 %all-gather.5.cloned.1.call-done = bf16[384,2048]{1,0:T(8,128)(2,1)} async-done(((bf16[384,512]{1,0:T(8,128)(2,1)}), bf16[384,2048]{1,0:T(8,128)(2,1)}) %all-gather.5.cloned.1.call-update) | async-done | bytes 1572880 | tf_op jit(solution)/shard_map/all_gather | solution.py:80
  33.1 2.6 %multiply_reduce_fusion.1 = (f32[384]{0:T(512)S(1)}, f32[384,256]{0,1:T(8,128)S(1)}) fusion(bf16[2048,256]{1,0:T(8,128)(2,1)} %param.25, bf16[384,2048]{1,0:T(8,128)(2,1)} %all-gather.5.cloned.1.call-done, f32[2048]{0:T(1024)} %param.21, f32[384]{0:T(512)S(1)} %add_rsqrt_fusion.4), kind=kOutput, calls=%fused_computation.112 | convolution fusion | flops 406191744 | bytes 3025920 | tf_op jit(solution)/shard_map/dot_general | solution.py:89
  38.3 2.6 %multiply_reduce_fusion = (f32[384]{0:T(512)S(1)}, f32[384,512]{1,0:T(8,128)S(1)}) fusion(bf16[2048,512]{1,0:T(8,128)(2,1)S(1)} %copy-done, bf16[384,2048]{1,0:T(8,128)(2,1)} %all-gather.5.cloned.1.call-done, f32[2048]{0:T(1024)S(1)} %copy-done.15, f32[384]{0:T(512)S(1)} %add_rsqrt_fusion.4), kind=kOutput, calls=%fused_computation.65 | convolution fusion | flops 809238144 | bytes 4467712 | tf_op jit(solution)/shard_map/dot_general | solution.py:82
  44.5 4.5 %collective-permute-start = (bf16[8,256]{1,0:T(8,128)(2,1)S(1)}, bf16[8,256]{1,0:T(8,128)(2,1)S(1)}, u32[]{:S(2)}, u32[]{:S(2)}) collective-permute-start(bf16[8,256]{1,0:T(8,128)(2,1)S(1)} %get-tuple-element.153), channel_id=1, source_target_pairs={{0,4},{4,8},{8,12},{12,16},{16,20},{20,24},{24,28},{1,5},{5,9},{9,... | collective-permute-start | bytes 12296 | tf_op jit(solution)/shard_map/ppermute | solution.py:23
  50.5 31.9 %all_gather.17 = bf16[3072,32]{0,1:T(8,128)(2,1)S(1)} all-gather(bf16[384,32]{0,1:T(8,128)(2,1)S(1)} %convolution_convert_fusion.7), channel_id=1, replica_groups=mesh['sp'=8,'tp'=4] {'sp'}, dimensions={0}, use_global_device_ids=true | all-gather | bytes 221184 | tf_op jit(solution)/shard_map/all_gather | solution.py:98
  85.3 4.0 %all-to-all-start.2 = ((bf16[4,96,256]{2,1,0:T(8,128)(2,1)}), bf16[4,96,256]{2,1,0:T(8,128)(2,1)}, u32[]{:S(2)}, u32[]{:S(2)}) async-start(bf16[4,96,256]{2,1,0:T(8,128)(2,1)} %multiply_convert_fusion.2), calls=%async_computation.2 | async-start | bytes 393216 | tf_op jit(solution)/shard_map/all_to_all | solution.py:166
  89.4 2.7 %copy.46 = bf16[3072,256]{1,0:T(8,128)(2,1)} copy(bf16[3072,256]{0,1:T(8,128)(2,1)} %all-gather.7.cloned.1.call-done) | data formatting | bytes 3145728
  92.1 73.3 %while.15 = (s32[]{:T(128)}, f32[4,384]{1,0:T(4,128)S(1)}, f32[4,384]{1,0:T(4,128)S(1)}, f32[4,384,64]{1,2,0:T(8,128)S(1)}, bf16[8,384,256]{2,1,0:T(8,128)(2,1)}...) while((s32[]{:T(128)}, f32[4,384]{1,0:T(4,128)S(1)}, ...), condition=%wide.region_8.9_spmd.clone, body=%wide.region_4.8_spmd.clone.sunk | while | flops 295714592 | bytes 23564012 | solution.py:130
  98.2 2.1 %fusion.99 = f32[4,384]{1,0:T(4,128)S(1)} fusion(f32[4,384,384]{2,1,0:T(8,128)} %get-tuple-element.235, f32[4,384]{1,0:T(4,128)S(1)} %select_maximum_fusion.2), kind=kLoop, calls=%fused_computation.4.clone.1 | loop fusion | flops 1178112 | bytes 2371584 | tf_op jit(solution)/shard_map/while/body/eval_jaxpr/reduce_sum | solution.py:124
  107.3 2.1 %fusion.99 = f32[4,384]{1,0:T(4,128)S(1)} fusion(f32[4,384,384]{2,1,0:T(8,128)} %get-tuple-element.235, f32[4,384]{1,0:T(4,128)S(1)} %select_maximum_fusion.2), kind=kLoop, calls=%fused_computation.4.clone.1 | loop fusion | flops 1178112 | bytes 2371584 | tf_op jit(solution)/shard_map/while/body/eval_jaxpr/reduce_sum | solution.py:124
  116.3 2.1 %fusion.99 = f32[4,384]{1,0:T(4,128)S(1)} fusion(f32[4,384,384]{2,1,0:T(8,128)} %get-tuple-element.235, f32[4,384]{1,0:T(4,128)S(1)} %select_maximum_fusion.2), kind=kLoop, calls=%fused_computation.4.clone.1 | loop fusion | flops 1178112 | bytes 2371584 | tf_op jit(solution)/shard_map/while/body/eval_jaxpr/reduce_sum | solution.py:124
  125.4 2.3 %fusion.99 = f32[4,384]{1,0:T(4,128)S(1)} fusion(f32[4,384,384]{2,1,0:T(8,128)} %get-tuple-element.235, f32[4,384]{1,0:T(4,128)S(1)} %select_maximum_fusion.2), kind=kLoop, calls=%fused_computation.4.clone.1 | loop fusion | flops 1178112 | bytes 2371584 | tf_op jit(solution)/shard_map/while/body/eval_jaxpr/reduce_sum | solution.py:124
  135.2 2.1 %fusion.99 = f32[4,384]{1,0:T(4,128)S(1)} fusion(f32[4,384,384]{2,1,0:T(8,128)} %get-tuple-element.235, f32[4,384]{1,0:T(4,128)S(1)} %select_maximum_fusion.2), kind=kLoop, calls=%fused_computation.4.clone.1 | loop fusion | flops 1178112 | bytes 2371584 | tf_op jit(solution)/shard_map/while/body/eval_jaxpr/reduce_sum | solution.py:124
  144.3 2.1 %fusion.99 = f32[4,384]{1,0:T(4,128)S(1)} fusion(f32[4,384,384]{2,1,0:T(8,128)} %get-tuple-element.235, f32[4,384]{1,0:T(4,128)S(1)} %select_maximum_fusion.2), kind=kLoop, calls=%fused_computation.4.clone.1 | loop fusion | flops 1178112 | bytes 2371584 | tf_op jit(solution)/shard_map/while/body/eval_jaxpr/reduce_sum | solution.py:124
  153.4 2.1 %fusion.99 = f32[4,384]{1,0:T(4,128)S(1)} fusion(f32[4,384,384]{2,1,0:T(8,128)} %get-tuple-element.235, f32[4,384]{1,0:T(4,128)S(1)} %select_maximum_fusion.2), kind=kLoop, calls=%fused_computation.4.clone.1 | loop fusion | flops 1178112 | bytes 2371584 | tf_op jit(solution)/shard_map/while/body/eval_jaxpr/reduce_sum | solution.py:124
  166.4 3.4 %all-to-all-start = ((bf16[4,96,256]{2,1,0:T(8,128)(2,1)}), bf16[4,96,256]{2,1,0:T(8,128)(2,1)S(1)}, u32[]{:S(2)}, u32[]{:S(2)}) async-start(bf16[4,96,256]{2,1,0:T(8,128)(2,1)} %copy.40), calls=%async_computation | async-start | bytes 393216 | tf_op jit(solution)/shard_map/all_to_all | solution.py:165
  170.8 4.4 %all-to-all-done = bf16[4,96,256]{2,1,0:T(8,128)(2,1)S(1)} async-done(((bf16[4,96,256]{2,1,0:T(8,128)(2,1)}), bf16[4,96,256]{2,1,0:T(8,128)(2,1)S(1)}, u32[]{:S(2)}, u32[]{:S(2)}) %all-to-all-start) | async-done | bytes 196640 | tf_op jit(solution)/shard_map/all_to_all | solution.py:165
  175.2 3.0 %convolution_convert_fusion.2 = bf16[96,2048]{1,0:T(8,128)(2,1)S(1)} fusion(bf16[96,1024]{1,0:T(8,128)(2,1)S(1)} %bitcast.121, bf16[1024,2048]{1,0:T(8,128)(2,1)} %all-gather.9.cloned.1.call-done), kind=kOutput, calls=%fused_computation.44 | convolution fusion | flops 402849792 | bytes 4784128 | tf_op jit(solution)/shard_map/dot_general | solution.py:172
  179.0 3.5 %all-to-all-start.1 = ((bf16[96,4,512]{2,0,1:T(8,128)(2,1)}), bf16[96,4,512]{2,0,1:T(8,128)(2,1)S(1)}, u32[]{:S(2)}, u32[]{:S(2)}) async-start(bf16[96,4,512]{2,0,1:T(8,128)(2,1)} %bitcast.93), calls=%async_computation.1 | async-start | bytes 786432 | tf_op jit(solution)/shard_map/all_to_all | solution.py:175
  182.5 3.0 %convolution_convert_fusion.1 = bf16[96,2048]{1,0:T(8,128)(2,1)S(1)} fusion(bf16[96,1024]{1,0:T(8,128)(2,1)S(1)} %bitcast.120, bf16[1024,2048]{1,0:T(8,128)(2,1)} %all-gather.11.cloned.1.call-done), kind=kOutput, calls=%fused_computation.43 | convolution fusion | flops 402849792 | bytes 4784128 | tf_op jit(solution)/shard_map/dot_general | solution.py:173
  186.3 3.6 %all-to-all-done.1 = bf16[96,4,512]{2,0,1:T(8,128)(2,1)S(1)} async-done(((bf16[96,4,512]{2,0,1:T(8,128)(2,1)}), bf16[96,4,512]{2,0,1:T(8,128)(2,1)S(1)}, u32[]{:S(2)}, u32[]{:S(2)}) %all-to-all-start.1) | async-done | bytes 393248 | tf_op jit(solution)/shard_map/all_to_all | solution.py:175
  189.8 3.5 %all-to-all-start.3 = ((bf16[96,4,512]{2,0,1:T(8,128)(2,1)}), bf16[96,4,512]{2,0,1:T(8,128)(2,1)S(1)}, u32[]{:S(2)}, u32[]{:S(2)}) async-start(bf16[96,4,512]{2,0,1:T(8,128)(2,1)} %bitcast.92), calls=%async_computation.3 | async-start | bytes 786432 | tf_op jit(solution)/shard_map/all_to_all | solution.py:178
  194.3 6.4 %all-to-all-done.3 = bf16[96,4,512]{2,0,1:T(8,128)(2,1)S(1)} async-done(((bf16[96,4,512]{2,0,1:T(8,128)(2,1)}), bf16[96,4,512]{2,0,1:T(8,128)(2,1)S(1)}, u32[]{:S(2)}, u32[]{:S(2)}) %all-to-all-start.3) | async-done | bytes 393248 | tf_op jit(solution)/shard_map/all_to_all | solution.py:178
  200.8 3.5 %fusion.26 = f32[384,512]{1,0:T(8,128)S(1)} fusion(f32[384,512]{1,0:T(8,128)} %bitcast.122, bf16[2048,512]{1,0:T(8,128)(2,1)} %param.36, bf16[384,2048]{1,0:T(8,128)(2,1)} %all-gather.5.cloned.1.call-done, f32[2048]{0:T(1024)S(1)} %copy-done.15, f32[384]{0:T(512)S(1)} %add_rsqrt_fusion.4), kind=kOutput, calls=%fused_computation.51 | convolution fusion | flops 809238528 | bytes 5252608 | tf_op jit(solution)/shard_map/dot_general | solution.py:162
  (265 shorter events, 71.3 us)
Async XLA Ops:
  6.5 31.7 %copy-start = (bf16[2048,512]{1,0:T(8,128)(2,1)S(1)}, bf16[2048,512]{1,0:T(8,128)(2,1)}, u32[]{:S(2)}) copy-start(bf16[2048,512]{1,0:T(8,128)(2,1)} %param.22) | copy-start | bytes 6291460
  6.5 24.7 %all-gather.5.cloned.1.call-start = ((), (), s32[]{:S(2)}) async-start(), calls=%async_computation.4 | async-start | bytes 1966080 | tf_op jit(solution)/shard_map/all_gather | solution.py:80
  7.3 82.1 %all-gather.7.cloned.1.call-start = ((), (), s32[]{:S(2)}) async-start(), calls=%async_computation.5 | async-start | bytes 1769472 | tf_op jit(solution)/shard_map/all_gather | solution.py:97
  33.1 2.6 %copy-start.8 = (f32[256]{0:T(256)S(1)}, f32[256]{0:T(256)}, u32[]{:S(2)}) copy-start(f32[256]{0:T(256)} %param.26) | copy-start | bytes 3076
  35.7 2.6 %copy-start.15 = (f32[2048]{0:T(1024)S(1)}, f32[2048]{0:T(1024)}, u32[]{:S(2)}) copy-start(f32[2048]{0:T(1024)} %param.21) | copy-start | bytes 24580
  36.5 138.7 %all-gather.9.cloned.1.call-start = ((), (), s32[]{:S(2)}) async-start(), calls=%async_computation.6 | async-start | bytes 5242880 | tf_op jit(solution)/shard_map/all_gather | solution.py:169
  37.3 145.2 %all-gather.11.cloned.1.call-start = ((), (), s32[]{:S(2)}) async-start(), calls=%async_computation.7 | async-start | bytes 5242880 | tf_op jit(solution)/shard_map/all_gather | solution.py:170
  38.3 2.6 %copy-start.5 = (bf16[512,384]{1,0:T(8,128)(2,1)S(1)}, bf16[512,384]{1,0:T(8,128)(2,1)}, u32[]{:S(2)}) copy-start(bf16[512,384]{1,0:T(8,128)(2,1)} %param.24) | copy-start | bytes 1179652
  38.3 2.6 %copy-start.7 = (f32[512]{0:T(512)S(1)}, f32[512]{0:T(512)}, u32[]{:S(2)}) copy-start(f32[512]{0:T(512)} %param.23) | copy-start | bytes 6148
  38.3 3.2 %copy-start.10 = (f32[96]{0:T(128)S(1)}, f32[96]{0:T(128)}, u32[]{:S(2)}) copy-start(f32[96]{0:T(128)} %param.29) | copy-start | bytes 1156
  42.6 7.3 %copy-start.13 = (bf16[2048,32]{0,1:T(8,128)(2,1)S(1)}, bf16[2048,32]{0,1:T(8,128)(2,1)}, u32[]{:S(2)}) copy-start(bf16[2048,32]{0,1:T(8,128)(2,1)} %param.27) | copy-start | bytes 393220
  43.2 39.9 %collective-permute-start.1 = (bf16[8,256]{1,0:T(8,128)(2,1)S(1)}, bf16[8,256]{1,0:T(8,128)(2,1)S(1)}, u32[]{:S(2)}, u32[]{:S(2)}) collective-permute-start(bf16[8,256]{1,0:T(8,128)(2,1)S(1)} %get-tuple-element.154), channel_id=1, source_target_pairs={{4,0},{8,4},{12,8},{16,12},{20,16},{24,20},{28,24},{5,1},{9,5},{13... | collective-permute-start | bytes 12296 | tf_op jit(solution)/shard_map/ppermute | solution.py:25
  44.5 38.6 %collective-permute-start = (bf16[8,256]{1,0:T(8,128)(2,1)S(1)}, bf16[8,256]{1,0:T(8,128)(2,1)S(1)}, u32[]{:S(2)}, u32[]{:S(2)}) collective-permute-start(bf16[8,256]{1,0:T(8,128)(2,1)S(1)} %get-tuple-element.153), channel_id=1, source_target_pairs={{0,4},{4,8},{8,12},{12,16},{16,20},{20,24},{24,28},{1,5},{5,9},{9,... | collective-permute-start | bytes 12296 | tf_op jit(solution)/shard_map/ppermute | solution.py:23
  49.1 34.1 %copy-start.14 = (bf16[1,256,256]{2,1,0:T(8,128)(2,1)S(1)}, bf16[1,256,256]{2,1,0:T(8,128)(2,1)}, u32[]{:S(2)}) copy-start(bf16[1,256,256]{2,1,0:T(8,128)(2,1)} %param.32) | copy-start | bytes 393220
  84.6 7.4 %copy-start.6 = (f32[96]{0:T(128)S(1)}, f32[96]{0:T(128)}, u32[]{:S(2)}) copy-start(f32[96]{0:T(128)} %param.30) | copy-start | bytes 1156
  85.3 81.1 %all-to-all-start.2 = ((bf16[4,96,256]{2,1,0:T(8,128)(2,1)}), bf16[4,96,256]{2,1,0:T(8,128)(2,1)}, u32[]{:S(2)}, u32[]{:S(2)}) async-start(bf16[4,96,256]{2,1,0:T(8,128)(2,1)} %multiply_convert_fusion.2), calls=%async_computation.2 | async-start | bytes 393216 | tf_op jit(solution)/shard_map/all_to_all | solution.py:166
  116.3 2.4 %copy-start.1 = (f32[4,384,384]{2,1,0:T(8,128)S(1)}, f32[4,384,384]{2,1,0:T(8,128)}, u32[]{:S(2)}) copy-start(f32[4,384,384]{2,1,0:T(8,128)} %get-tuple-element.235) | copy-start | bytes 7077892 | tf_op jit(solution)/shard_map/while
  125.4 3.1 %copy-start.1 = (f32[4,384,384]{2,1,0:T(8,128)S(1)}, f32[4,384,384]{2,1,0:T(8,128)}, u32[]{:S(2)}) copy-start(f32[4,384,384]{2,1,0:T(8,128)} %get-tuple-element.235) | copy-start | bytes 7077892 | tf_op jit(solution)/shard_map/while
  135.2 2.4 %copy-start.1 = (f32[4,384,384]{2,1,0:T(8,128)S(1)}, f32[4,384,384]{2,1,0:T(8,128)}, u32[]{:S(2)}) copy-start(f32[4,384,384]{2,1,0:T(8,128)} %get-tuple-element.235) | copy-start | bytes 7077892 | tf_op jit(solution)/shard_map/while
  166.4 8.7 %all-to-all-start = ((bf16[4,96,256]{2,1,0:T(8,128)(2,1)}), bf16[4,96,256]{2,1,0:T(8,128)(2,1)S(1)}, u32[]{:S(2)}, u32[]{:S(2)}) async-start(bf16[4,96,256]{2,1,0:T(8,128)(2,1)} %copy.40), calls=%async_computation | async-start | bytes 393216 | tf_op jit(solution)/shard_map/all_to_all | solution.py:165
  179.0 10.8 %all-to-all-start.1 = ((bf16[96,4,512]{2,0,1:T(8,128)(2,1)}), bf16[96,4,512]{2,0,1:T(8,128)(2,1)S(1)}, u32[]{:S(2)}, u32[]{:S(2)}) async-start(bf16[96,4,512]{2,0,1:T(8,128)(2,1)} %bitcast.93), calls=%async_computation.1 | async-start | bytes 786432 | tf_op jit(solution)/shard_map/all_to_all | solution.py:175
  189.8 10.8 %all-to-all-start.3 = ((bf16[96,4,512]{2,0,1:T(8,128)(2,1)}), bf16[96,4,512]{2,0,1:T(8,128)(2,1)S(1)}, u32[]{:S(2)}, u32[]{:S(2)}) async-start(bf16[96,4,512]{2,0,1:T(8,128)(2,1)} %bitcast.92), calls=%async_computation.3 | async-start | bytes 786432 | tf_op jit(solution)/shard_map/all_to_all | solution.py:178
  200.7 3.6 %copy-start.4 = (bf16[384,2048]{1,0:T(8,128)(2,1)S(1)}, bf16[384,2048]{1,0:T(8,128)(2,1)}, u32[]{:S(2)}) copy-start(bf16[384,2048]{1,0:T(8,128)(2,1)} %all-gather.5.cloned.1.call-done) | copy-start | bytes 4718596
  200.8 3.6 %copy-start.11 = (bf16[2048,512]{1,0:T(8,128)(2,1)S(1)}, bf16[2048,512]{1,0:T(8,128)(2,1)}, u32[]{:S(2)}) copy-start(bf16[2048,512]{1,0:T(8,128)(2,1)} %param.37) | copy-start | bytes 6291460
  (16 other events, 31.0 us)
Sparse Core Ops, SparseCore 0:
  8.9 22.3 all-gather.4
  36.6 45.9 all-gather.6
  84.2 34.4 all-gather.8
  120.1 32.7 all-gather.10
where the time goes:
time: 214 us; the launch traced here: 213 us
  matrix products  50.5 us (24%)
  waiting for transfers between devices  40.3 us (19%)
  blocking collectives  31.9 us (15%)
  other arithmetic  26.5 us (12%)
  local copies, waits for them, and re-layouts  23.5 us (11%)
  starting transfers between devices  20.3 us (9%)
  between operations  13.7 us (6%)
  loops' own time  6.1 us (3%)
    all_gather x1, blocking collectives, body(): rotary_piece = lax.all_gather(rotary_key, 'sp', axis=0, tiled=True)  31.9 us
    all_gather x1, waiting for transfers between devices, body(): whole = lax.all_gather(tokens, 'tp', axis=1, tiled=True)  24 us
    reduce_sum x8, other arithmetic, one_block(): total = total * factor + jnp.sum(expo, axis=-1)  17.4 us
    dot_general x8, matrix products, one_block(): jnp.einsum('qhd,khd->hqk', query, key, preferred_element_type=jnp.float32)  16 us
    dot_general x8, matrix products, one_block(): jnp.dot(latent_block, w_latent_up, preferred_element_type=jnp.float32)  10.5 us
    all_to_all x1, waiting for transfers between devices, body(): lax.all_to_all(pool_here.astype(jnp.bfloat16), 'tp', split_axis=1, concat...  6.4 us
    another operation x1, loops' own time, body(): lax.scan(one_block, start_state, (latent_blocks, rotary_blocks, jnp.arang...  6.1 us
    broadcast_in_dim x16, local copies, waits for them, and re-layouts, one_block(): jnp.broadcast_to(rotary_block[:, None, :], (rows, local_heads, ROPE))  6.05 us
  transfers between devices with their start and end apart: 10, of which 4 were waited for; matrix products, arithmetic and copies ran while one was open for 41% of the time, Pallas kernels for 0%

commit v1 on v0

--- a/solution.py
+++ b/solution.py
@@ -2,6 +2,7 @@
 import jax.numpy as jnp
 from jax import lax
 from jax.sharding import PartitionSpec as P
+from jax.lax import all_gather
 
 NOPE = 64
 ROPE = 32
@@ -77,7 +78,10 @@
     length = rows * lax.axis_size("sp")
     local_heads = w_query_up.shape[1] // (NOPE + ROPE)
     positions = lax.axis_index("sp") * rows + jnp.arange(rows, dtype=jnp.int32)
-    whole = lax.all_gather(tokens, "tp", axis=1, tiled=True)
+    read_the_terms = lambda panel, which_axis, axis_k: jnp.concatenate(
+        all_gather(panel, which_axis), axis=axis_k
+    )
+    whole = read_the_terms(tokens, which_axis="tp", axis_k=1)
     normed = rms_scale(whole, norm_gain).astype(bf)
     query_latent = jnp.dot(normed, w_query_down, preferred_element_type=jnp.float32).astype(bf)
     query_normed = rms_scale(query_latent, query_gain).astype(bf)

time: 214 us -> 229 us (1.070)
  other arithmetic: 26.5 us -> 37.1 us
  local copies, waits for them, and re-layouts: 23.5 us -> 31.8 us
  waiting for transfers between devices: 40.3 us -> 37 us
    convert_element_type x0 -> x2, other arithmetic: none -> 5.94 us  [the longest x1 3.59 us: rms_scale(): values = values.astype(jnp.float32)]
    mul x9, other arithmetic: 0.98 us -> 6.25 us  [rms_scale(): values * lax.rsqrt(jnp.mean(values * values, axis=-1, keepdims=True) + eps)]
    dynamic_slice x8, local copies, waits for them, and re-layouts: 5.25 us -> 9.91 us  [body(): lax.scan(one_block, start_state, (latent_blocks, rotary_blocks, jnp.arang...]
    convert_element_type x0 -> x1, local copies, waits for them, and re-layouts: none -> 3.58 us  [rms_scale(): values = values.astype(jnp.float32)]
    all_to_all x1, waiting for transfers between devices: 6.4 us -> 3.18 us  [body(): lax.all_to_all(pool_here.astype(jnp.bfloat16), 'tp', split_axis=1, concat...]
  transfers between devices with their start and end apart: 10 -> 10, of which waited for: 4 -> 4; matrix products, arithmetic and copies ran while one was open for 41% -> 44% of each run, Pallas kernels for 0% -> 0%
where the time goes in v1:
time: 229 us; the launch traced here: 228 us
  matrix products  49.9 us (22%)
  other arithmetic  37.1 us (16%)
  waiting for transfers between devices  37 us (16%)
  blocking collectives  33.5 us (15%)
  local copies, waits for them, and re-layouts  31.8 us (14%)
  starting transfers between devices  19.2 us (8%)
  between operations  13.7 us (6%)
  loops' own time  5.65 us (2%)
    all_gather x1, blocking collectives, body(): rotary_piece = lax.all_gather(rotary_key, 'sp', axis=0, tiled=True)  33.5 us
    all_gather x1, waiting for transfers between devices, body(): all_gather(panel, which_axis)  24 us
    reduce_sum x8, other arithmetic, one_block(): total = total * factor + jnp.sum(expo, axis=-1)  17.1 us
    dot_general x8, matrix products, one_block(): jnp.einsum('qhd,khd->hqk', query, key, preferred_element_type=jnp.float32)  15.8 us
    dynamic_slice x8, local copies, waits for them, and re-layouts, body(): lax.scan(one_block, start_state, (latent_blocks, rotary_blocks, jnp.arang...  9.91 us
    dot_general x8, matrix products, one_block(): jnp.dot(latent_block, w_latent_up, preferred_element_type=jnp.float32)  9.5 us
    broadcast_in_dim x16, local copies, waits for them, and re-layouts, one_block(): jnp.broadcast_to(rotary_block[:, None, :], (rows, local_heads, ROPE))  6.38 us
    mul x9, other arithmetic, rms_scale(): values * lax.rsqrt(jnp.mean(values * values, axis=-1, keepdims=True) + eps)  6.25 us
  transfers between devices with their start and end apart: 10, of which 4 were waited for; matrix products, arithmetic and copies ran while one was open for 44% of the time, Pallas kernels for 0%

profile of v1, /device:TPU:0, one launch (start us, length us, event | category | flops | bytes accessed | tf_op | source)
XLA Modules:
  0.0 227.9 jit_solution(17712845649548550093)
XLA Ops:
  7.3 24.0 %all-gather.12.cloned.1.call-done = bf16[1536,512]{1,0:T(8,128)(2,1)} async-done(((bf16[384,512]{1,0:T(8,128)(2,1)}), bf16[1536,512]{1,0:T(8,128)(2,1)}) %all-gather.12.cloned.1.call-update) | async-done | bytes 1572880 | tf_op jit(solution)/shard_map/all_gather | solution.py:82
  31.3 3.6 %convert_bitcast_fusion = f32[384,4,512]{2,0,1:T(8,128)} fusion(bf16[4,384,512]{2,1,0:T(8,128)(2,1)} %bitcast.131), kind=kLoop, calls=%fused_computation.39 | loop fusion | flops 786432 | bytes 4718592 | tf_op jit(solution)/shard_map/convert_element_type | solution.py:34
  35.3 3.6 %copy.48 = f32[384,4,512]{0,2,1:T(8,128)} copy(f32[384,4,512]{2,0,1:T(8,128)} %convert_bitcast_fusion) | data formatting | bytes 6291456 | tf_op jit(solution)/shard_map/convert_element_type | solution.py:34
  38.9 2.3 %fusion.21 = bf16[384,2048]{0,1:T(8,128)(2,1)S(1)} fusion(f32[384,4,512]{0,2,1:T(8,128)} %copy.48, f32[2048]{0:T(1024)S(1)} %copy-done.12, f32[384]{0:T(512)S(1)} %add_rsqrt_fusion.4), kind=kLoop, calls=%fused_computation.43 | loop fusion | flops 2359296 | bytes 4728320 | tf_op jit(solution)/shard_map/convert_element_type | solution.py:85
  48.3 3.4 %collective-permute-start = (bf16[8,256]{1,0:T(8,128)(2,1)S(1)}, bf16[8,256]{1,0:T(8,128)(2,1)S(1)}, u32[]{:S(2)}, u32[]{:S(2)}) collective-permute-start(bf16[8,256]{1,0:T(8,128)(2,1)S(1)} %get-tuple-element.163), channel_id=1, source_target_pairs={{0,4},{4,8},{8,12},{12,16},{16,20},{20,24},{24,28},{1,5},{5,9},{9,... | collective-permute-start | bytes 12296 | tf_op jit(solution)/shard_map/ppermute | solution.py:24
  56.3 33.5 %all_gather.21 = bf16[3072,32]{0,1:T(8,128)(2,1)S(1)} all-gather(bf16[384,32]{0,1:T(8,128)(2,1)S(1)} %convolution_convert_fusion.7), channel_id=1, replica_groups=mesh['sp'=8,'tp'=4] {'sp'}, dimensions={0}, use_global_device_ids=true | all-gather | bytes 221184 | tf_op jit(solution)/shard_map/all_gather | solution.py:102
  92.7 4.0 %all-to-all-start.2 = ((bf16[4,96,256]{2,1,0:T(8,128)(2,1)}), bf16[4,96,256]{2,1,0:T(8,128)(2,1)}, u32[]{:S(2)}, u32[]{:S(2)}) async-start(bf16[4,96,256]{2,1,0:T(8,128)(2,1)} %multiply_convert_fusion.2), calls=%async_computation.2 | async-start | bytes 393216 | tf_op jit(solution)/shard_map/all_to_all | solution.py:170
  96.7 2.7 %copy.57 = bf16[3072,256]{1,0:T(8,128)(2,1)} copy(bf16[3072,256]{0,1:T(8,128)(2,1)} %all-gather.6.cloned.1.call-done) | data formatting | bytes 3145728
  100.0 81.2 %while.15 = (s32[]{:T(128)}, f32[4,384]{1,0:T(4,128)S(1)}, f32[4,384]{1,0:T(4,128)}, f32[4,384,64]{1,2,0:T(8,128)S(1)}, bf16[8,384,256]{2,1,0:T(8,128)(2,1)}, /*...) while((s32[]{:T(128)}, f32[4,384]{1,0:T(4,128)S(1)}, ...), condition=%wide.region_8.9_spmd.clone, body=%wide.region_4.8_spmd.clone.sunk | while | flops 295714592 | bytes 23613720 | solution.py:134
  107.2 2.1 fusion.99
  117.4 2.1 fusion.99
  127.5 2.1 fusion.99
  137.7 2.1 fusion.99
  178.3 2.1 fusion.99
  183.0 3.4 %all-to-all-start = ((bf16[4,96,256]{2,1,0:T(8,128)(2,1)}), bf16[4,96,256]{2,1,0:T(8,128)(2,1)S(1)}, u32[]{:S(2)}, u32[]{:S(2)}) async-start(bf16[4,96,256]{2,1,0:T(8,128)(2,1)} %copy.51), calls=%async_computation | async-start | bytes 393216 | tf_op jit(solution)/shard_map/all_to_all | solution.py:169
  187.3 4.3 %all-to-all-done = bf16[4,96,256]{2,1,0:T(8,128)(2,1)S(1)} async-done(((bf16[4,96,256]{2,1,0:T(8,128)(2,1)}), bf16[4,96,256]{2,1,0:T(8,128)(2,1)S(1)}, u32[]{:S(2)}, u32[]{:S(2)}) %all-to-all-start) | async-done | bytes 196640 | tf_op jit(solution)/shard_map/all_to_all | solution.py:169
  191.7 3.0 %convolution_convert_fusion.2 = bf16[96,2048]{1,0:T(8,128)(2,1)S(1)} fusion(bf16[96,1024]{1,0:T(8,128)(2,1)S(1)} %bitcast.139, bf16[1024,2048]{1,0:T(8,128)(2,1)} %all-gather.8.cloned.1.call-done), kind=kOutput, calls=%fused_computation.45 | convolution fusion | flops 402849792 | bytes 4784128 | tf_op jit(solution)/shard_map/dot_general | solution.py:176
  195.5 3.5 %all-to-all-start.1 = ((bf16[96,4,512]{2,0,1:T(8,128)(2,1)}), bf16[96,4,512]{2,0,1:T(8,128)(2,1)S(1)}, u32[]{:S(2)}, u32[]{:S(2)}) async-start(bf16[96,4,512]{2,0,1:T(8,128)(2,1)} %bitcast.109), calls=%async_computation.1 | async-start | bytes 786432 | tf_op jit(solution)/shard_map/all_to_all | solution.py:179
  199.0 3.0 %convolution_convert_fusion.1 = bf16[96,2048]{1,0:T(8,128)(2,1)S(1)} fusion(bf16[96,1024]{1,0:T(8,128)(2,1)S(1)} %bitcast.138, bf16[1024,2048]{1,0:T(8,128)(2,1)} %all-gather.10.cloned.1.call-done), kind=kOutput, calls=%fused_computation.44 | convolution fusion | flops 402849792 | bytes 4784128 | tf_op jit(solution)/shard_map/dot_general | solution.py:177
  202.8 3.6 %all-to-all-done.1 = bf16[96,4,512]{2,0,1:T(8,128)(2,1)S(1)} async-done(((bf16[96,4,512]{2,0,1:T(8,128)(2,1)}), bf16[96,4,512]{2,0,1:T(8,128)(2,1)S(1)}, u32[]{:S(2)}, u32[]{:S(2)}) %all-to-all-start.1) | async-done | bytes 393248 | tf_op jit(solution)/shard_map/all_to_all | solution.py:179
  206.3 3.5 %all-to-all-start.3 = ((bf16[96,4,512]{2,0,1:T(8,128)(2,1)}), bf16[96,4,512]{2,0,1:T(8,128)(2,1)S(1)}, u32[]{:S(2)}, u32[]{:S(2)}) async-start(bf16[96,4,512]{2,0,1:T(8,128)(2,1)} %bitcast.108), calls=%async_computation.3 | async-start | bytes 786432 | tf_op jit(solution)/shard_map/all_to_all | solution.py:182
  209.9 4.1 %fusion.26 = f32[384,512]{1,0:T(8,128)} fusion(f32[384,512]{1,0:T(8,128)S(1)} %bitcast.141, bf16[384,2048]{0,1:T(8,128)(2,1)} %copy-done.2, bf16[2048,512]{1,0:T(8,128)(2,1)} %param.36), kind=kOutput, calls=%fused_computation.52 | convolution fusion | flops 806092800 | bytes 5242880 | tf_op jit(solution)/shard_map/dot_general | solution.py:166
  214.0 3.2 %all-to-all-done.3 = bf16[96,4,512]{2,0,1:T(8,128)(2,1)S(1)} async-done(((bf16[96,4,512]{2,0,1:T(8,128)(2,1)}), bf16[96,4,512]{2,0,1:T(8,128)(2,1)S(1)}, u32[]{:S(2)}, u32[]{:S(2)}) %all-to-all-start.3) | async-done | bytes 393248 | tf_op jit(solution)/shard_map/all_to_all | solution.py:182
  217.3 4.1 %fusion.31 = bf16[384,512]{1,0:T(8,128)(2,1)} fusion(f32[384,512]{1,0:T(8,128)} %fusion.26, f32[384,512]{1,0:T(8,128)S(1)} %bitcast.140, bf16[384,2048]{0,1:T(8,128)(2,1)} %copy-done.2, bf16[2048,512]{1,0:T(8,128)(2,1)} %param.37), kind=kOutput, calls=%fused_computation.57 | convolution fusion | flops 806486016 | bytes 5636096 | tf_op jit(solution)/shard_map/dot_general | solution.py:167
  (302 shorter events, 85.3 us)
Async XLA Ops:
  6.5 46.6 %copy-start = (bf16[2048,512]{1,0:T(8,128)(2,1)S(1)}, bf16[2048,512]{1,0:T(8,128)(2,1)}, u32[]{:S(2)}) copy-start(bf16[2048,512]{1,0:T(8,128)(2,1)} %param.22) | copy-start | bytes 6291460
  6.5 24.7 %all-gather.12.cloned.1.call-start = ((), (), s32[]{:S(2)}) async-start(), calls=%async_computation.7 | async-start | bytes 1966080 | tf_op jit(solution)/shard_map/all_gather | solution.py:82
  7.3 89.5 %all-gather.6.cloned.1.call-start = ((), (), s32[]{:S(2)}) async-start(), calls=%async_computation.4 | async-start | bytes 1769472 | tf_op jit(solution)/shard_map/all_gather | solution.py:101
  31.3 3.6 %copy-start.6 = (bf16[1536,512]{1,0:T(8,128)(2,1)S(1)}, bf16[1536,512]{1,0:T(8,128)(2,1)}, u32[]{:S(2)}) copy-start(bf16[1536,512]{1,0:T(8,128)(2,1)} %all-gather.12.cloned.1.call-done) | copy-start | bytes 4718596
  42.4 3.8 %copy-start.7 = (bf16[2048,256]{1,0:T(8,128)(2,1)S(1)}, bf16[2048,256]{1,0:T(8,128)(2,1)}, u32[]{:S(2)}) copy-start(bf16[2048,256]{1,0:T(8,128)(2,1)} %param.31) | copy-start | bytes 3145732
  43.2 148.5 %all-gather.8.cloned.1.call-start = ((), (), s32[]{:S(2)}) async-start(), calls=%async_computation.5 | async-start | bytes 5242880 | tf_op jit(solution)/shard_map/all_gather | solution.py:173
  44.0 155.0 %all-gather.10.cloned.1.call-start = ((), (), s32[]{:S(2)}) async-start(), calls=%async_computation.6 | async-start | bytes 5242880 | tf_op jit(solution)/shard_map/all_gather | solution.py:174
  45.2 7.9 %copy-start.3 = (bf16[384,2048]{0,1:T(8,128)(2,1)S(1)}, bf16[384,2048]{0,1:T(8,128)(2,1)}, u32[]{:S(2)}) copy-start(bf16[384,2048]{0,1:T(8,128)(2,1)} %copy-done.2) | copy-start | bytes 4718596
  48.3 42.2 %collective-permute-start = (bf16[8,256]{1,0:T(8,128)(2,1)S(1)}, bf16[8,256]{1,0:T(8,128)(2,1)S(1)}, u32[]{:S(2)}, u32[]{:S(2)}) collective-permute-start(bf16[8,256]{1,0:T(8,128)(2,1)S(1)} %get-tuple-element.163), channel_id=1, source_target_pairs={{0,4},{4,8},{8,12},{12,16},{16,20},{20,24},{24,28},{1,5},{5,9},{9,... | collective-permute-start | bytes 12296 | tf_op jit(solution)/shard_map/ppermute | solution.py:24
  51.7 38.8 %collective-permute-start.1 = (bf16[8,256]{1,0:T(8,128)(2,1)S(1)}, bf16[8,256]{1,0:T(8,128)(2,1)S(1)}, u32[]{:S(2)}, u32[]{:S(2)}) collective-permute-start(bf16[8,256]{1,0:T(8,128)(2,1)S(1)} %get-tuple-element.164), channel_id=1, source_target_pairs={{4,0},{8,4},{12,8},{16,12},{20,16},{24,20},{28,24},{5,1},{9,5},{13... | collective-permute-start | bytes 12296 | tf_op jit(solution)/shard_map/ppermute | solution.py:26
  55.2 35.4 %copy-start.18 = (bf16[1,256,256]{2,1,0:T(8,128)(2,1)S(1)}, bf16[1,256,256]{2,1,0:T(8,128)(2,1)}, u32[]{:S(2)}) copy-start(bf16[1,256,256]{2,1,0:T(8,128)(2,1)} %param.32) | copy-start | bytes 393220
  92.0 8.1 %copy-start.5 = (bf16[256,512]{1,0:T(8,128)(2,1)S(1)}, bf16[256,512]{1,0:T(8,128)(2,1)}, u32[]{:S(2)}) copy-start(bf16[256,512]{1,0:T(8,128)(2,1)} %param.28) | copy-start | bytes 786436
  92.7 90.3 %all-to-all-start.2 = ((bf16[4,96,256]{2,1,0:T(8,128)(2,1)}), bf16[4,96,256]{2,1,0:T(8,128)(2,1)}, u32[]{:S(2)}, u32[]{:S(2)}) async-start(bf16[4,96,256]{2,1,0:T(8,128)(2,1)} %multiply_convert_fusion.2), calls=%async_computation.2 | async-start | bytes 393216 | tf_op jit(solution)/shard_map/all_to_all | solution.py:170
  101.4 3.8 %copy-start.4 = (bf16[384,4,96]{0,2,1:T(8,128)(2,1)S(1)}, bf16[384,4,96]{0,2,1:T(8,128)(2,1)}, u32[]{:S(2)}) copy-start(bf16[384,4,96]{0,2,1:T(8,128)(2,1)} %get-tuple-element.283) | copy-start | bytes 884740 | tf_op jit(solution)/shard_map/while
  111.6 3.8 %copy-start.4 = (bf16[384,4,96]{0,2,1:T(8,128)(2,1)S(1)}, bf16[384,4,96]{0,2,1:T(8,128)(2,1)}, u32[]{:S(2)}) copy-start(bf16[384,4,96]{0,2,1:T(8,128)(2,1)} %get-tuple-element.283) | copy-start | bytes 884740 | tf_op jit(solution)/shard_map/while
  121.8 3.8 %copy-start.4 = (bf16[384,4,96]{0,2,1:T(8,128)(2,1)S(1)}, bf16[384,4,96]{0,2,1:T(8,128)(2,1)}, u32[]{:S(2)}) copy-start(bf16[384,4,96]{0,2,1:T(8,128)(2,1)} %get-tuple-element.283) | copy-start | bytes 884740 | tf_op jit(solution)/shard_map/while
  131.9 3.8 %copy-start.4 = (bf16[384,4,96]{0,2,1:T(8,128)(2,1)S(1)}, bf16[384,4,96]{0,2,1:T(8,128)(2,1)}, u32[]{:S(2)}) copy-start(bf16[384,4,96]{0,2,1:T(8,128)(2,1)} %get-tuple-element.283) | copy-start | bytes 884740 | tf_op jit(solution)/shard_map/while
  142.1 3.8 %copy-start.4 = (bf16[384,4,96]{0,2,1:T(8,128)(2,1)S(1)}, bf16[384,4,96]{0,2,1:T(8,128)(2,1)}, u32[]{:S(2)}) copy-start(bf16[384,4,96]{0,2,1:T(8,128)(2,1)} %get-tuple-element.283) | copy-start | bytes 884740 | tf_op jit(solution)/shard_map/while
  152.3 3.8 %copy-start.4 = (bf16[384,4,96]{0,2,1:T(8,128)(2,1)S(1)}, bf16[384,4,96]{0,2,1:T(8,128)(2,1)}, u32[]{:S(2)}) copy-start(bf16[384,4,96]{0,2,1:T(8,128)(2,1)} %get-tuple-element.283) | copy-start | bytes 884740 | tf_op jit(solution)/shard_map/while
  162.4 3.8 %copy-start.4 = (bf16[384,4,96]{0,2,1:T(8,128)(2,1)S(1)}, bf16[384,4,96]{0,2,1:T(8,128)(2,1)}, u32[]{:S(2)}) copy-start(bf16[384,4,96]{0,2,1:T(8,128)(2,1)} %get-tuple-element.283) | copy-start | bytes 884740 | tf_op jit(solution)/shard_map/while
  172.5 3.8 %copy-start.4 = (bf16[384,4,96]{0,2,1:T(8,128)(2,1)S(1)}, bf16[384,4,96]{0,2,1:T(8,128)(2,1)}, u32[]{:S(2)}) copy-start(bf16[384,4,96]{0,2,1:T(8,128)(2,1)} %get-tuple-element.283) | copy-start | bytes 884740 | tf_op jit(solution)/shard_map/while
  183.0 8.6 %all-to-all-start = ((bf16[4,96,256]{2,1,0:T(8,128)(2,1)}), bf16[4,96,256]{2,1,0:T(8,128)(2,1)S(1)}, u32[]{:S(2)}, u32[]{:S(2)}) async-start(bf16[4,96,256]{2,1,0:T(8,128)(2,1)} %copy.51), calls=%async_computation | async-start | bytes 393216 | tf_op jit(solution)/shard_map/all_to_all | solution.py:169
  195.5 10.8 %all-to-all-start.1 = ((bf16[96,4,512]{2,0,1:T(8,128)(2,1)}), bf16[96,4,512]{2,0,1:T(8,128)(2,1)S(1)}, u32[]{:S(2)}, u32[]{:S(2)}) async-start(bf16[96,4,512]{2,0,1:T(8,128)(2,1)} %bitcast.109), calls=%async_computation.1 | async-start | bytes 786432 | tf_op jit(solution)/shard_map/all_to_all | solution.py:179
  206.3 10.8 %all-to-all-start.3 = ((bf16[96,4,512]{2,0,1:T(8,128)(2,1)}), bf16[96,4,512]{2,0,1:T(8,128)(2,1)S(1)}, u32[]{:S(2)}, u32[]{:S(2)}) async-start(bf16[96,4,512]{2,0,1:T(8,128)(2,1)} %bitcast.108), calls=%async_computation.3 | async-start | bytes 786432 | tf_op jit(solution)/shard_map/all_to_all | solution.py:182
  (33 other events, 61.6 us)
Sparse Core Ops, SparseCore 0:
  8.9 22.3 all-gather.11
  43.4 46.0 all-gather.5
  91.0 35.0 all-gather.7
  127.5 33.5 all-gather.9
